TPU v7x, 32 devices: a whole 2x2x4 slice. The times are simulated.
32 devices in a mesh: sp: 4 (over y, x), tp: 8 (over z, core).
Axes of the slice: x: 2, y: 2, z: 4, core: 2. Of those that a mesh axis runs over, the one named last changes fastest.
Arguments:
- latent: bfloat16 [4096, 2048], P(('sp', 'tp')), may hold values from -1.5 to 1.5
- context: bfloat16 [128, 2048], P('sp'), may hold values from -6 to 6
- cond: bfloat16 [2048], replicated, may hold values from -6 to 6
- cond_context: bfloat16 [2048], replicated, may hold values from -6 to 6
- mod_weight: bfloat16 [3, 2048, 2048], P(None, 'sp', 'tp'), may hold values from -0.125 to 0.125
- norm_gain: bfloat16 [2048], replicated, may hold values from 0.099609375 to 1.8984375
- down_q: bfloat16 [2048, 768], P('tp'), may hold values from -0.125 to 0.125
- down_kv: bfloat16 [2048, 512], P('tp'), may hold values from -0.125 to 0.125
- rope_weight: bfloat16 [2048, 32], replicated, may hold values from -0.125 to 0.125
- qlat_gain: bfloat16 [768], replicated, may hold values from 0.099609375 to 1.8984375
- kvlat_gain: bfloat16 [512], replicated, may hold values from 0.099609375 to 1.8984375
- up_query: bfloat16 [768, 1536], P(None, 'tp'), may hold values from -0.21875 to 0.21875
- up_key: bfloat16 [512, 1024], P(None, 'tp'), may hold values from -0.25 to 0.25
- up_value: bfloat16 [512, 1024], P(None, 'tp'), may hold values from -0.25 to 0.25
- query_gain: float32 [96], replicated, may hold values from 0.5 to 8
- key_gain: float32 [96], replicated, may hold values from 0.5 to 8
- context_bias: float32 [16], P('tp'), may hold values from -2.2 to -0.7
- out_weight: bfloat16 [1024, 2048], P('tp'), may hold values from -24 to 24
Outputs:
- mixed: bfloat16 [4096, 2048], P(('sp', 'tp'))
All inputs are finite; a program needn't handle non-finite values.
Results may differ from a plain program's by a relative error of at most 0.028.
The roundings to bfloat16 on the way count: a program that leaves them out, or rounds other values in their place, can miss the bound.
Values may be sent and summed in bfloat16 or wider, within the bound.
A program may use at most 64 MiB of HBM per device.

v0:
```python
import math
import jax
import jax.numpy as jnp
from jax import lax
from jax.sharding import PartitionSpec as P

NOPE = 64
ROPE = 32
VDIM = 64
GRID_W = 64
TOK_DEV = 1024
CTX_DEV = 32
epsilon = 1e-06
theta = 10000.0


def rms_scale(tensor, gain):
    return (
        tensor
        * lax.rsqrt(jnp.mean(tensor * tensor, axis=-1, keepdims=True) + epsilon)
        * gain.astype(jnp.float32)
    )


def axial_tables(positions):
    pair_count = ROPE // 4
    frequency = jnp.power(theta, -jnp.arange(pair_count, dtype=jnp.float32) / pair_count)
    row_angle = (positions // GRID_W).astype(jnp.float32)[:, None] * frequency
    col_angle = (positions % GRID_W).astype(jnp.float32)[:, None] * frequency
    return (jnp.cos(row_angle), jnp.sin(row_angle), jnp.cos(col_angle), jnp.sin(col_angle))


def rotate_half(tensor, cosine, sine_table):
    first, second = jnp.split(tensor, 2, axis=-1)
    cosine = cosine[:, None, :]
    sine_table = sine_table[:, None, :]
    return jnp.concatenate(
        [first * cosine - second * sine_table, second * cosine + first * sine_table], axis=-1
    )


def axial_rotate(tensor, tables):
    half_width = tensor.shape[-1] // 2
    return jnp.concatenate(
        [
            rotate_half(tensor[..., :half_width], tables[0], tables[1]),
            rotate_half(tensor[..., half_width:], tables[2], tables[3]),
        ],
        axis=-1,
    )


def modulate(row_block, gain, shifts, scales):
    normal = rms_scale(row_block.astype(jnp.float32), gain)
    return (normal * (1.0 + scales) + shifts).astype(jnp.bfloat16)


def make_queries(query_latent, up_query, query_gain, tables):
    amount = query_latent.shape[0]
    projected = jnp.dot(query_latent, up_query, preferred_element_type=jnp.float32).reshape(
        amount, -1, NOPE + ROPE
    )
    normal = rms_scale(projected, query_gain)
    return jnp.concatenate(
        [normal[..., :NOPE], axial_rotate(normal[..., NOPE:], tables)], axis=-1
    ).astype(jnp.bfloat16)


def make_keys(kv_latent, rope_rows, up_key, up_value, key_gain, tables):
    amount = kv_latent.shape[0]
    unrotated = jnp.dot(kv_latent, up_key, preferred_element_type=jnp.float32).reshape(
        amount, -1, NOPE
    )
    head_count = unrotated.shape[1]
    shared = jnp.broadcast_to(rope_rows.astype(jnp.float32)[:, None, :], (amount, head_count, ROPE))
    normal = rms_scale(jnp.concatenate([unrotated, shared], axis=-1), key_gain)
    if tables is not None:
        normal = jnp.concatenate(
            [normal[..., :NOPE], axial_rotate(normal[..., NOPE:], tables)], axis=-1
        )
    values = jnp.dot(kv_latent, up_value, preferred_element_type=jnp.float32).reshape(
        amount, head_count, VDIM
    )
    return (normal.astype(jnp.bfloat16), values.astype(jnp.bfloat16))


def absorb_block(state_in, queries, key_block, value_block, shift_heads):
    run_max, run_sum, run_acc = state_in
    scores = jnp.einsum("qhd,khd->qhk", queries, key_block, preferred_element_type=jnp.float32) * (
        NOPE + ROPE
    ) ** (-0.5)
    scores = scores + shift_heads[None, :, None]
    new_max = jnp.maximum(run_max, jnp.max(scores, axis=-1))
    factor = jnp.exp(run_max - new_max)
    weights = jnp.exp(scores - new_max[..., None])
    run_sum = run_sum * factor + jnp.sum(weights, axis=-1)
    run_acc = run_acc * factor[..., None] + jnp.einsum(
        "qhk,khd->qhd",
        weights.astype(jnp.bfloat16),
        value_block,
        preferred_element_type=jnp.float32,
    )
    return (new_max, run_sum, run_acc)


def shards(
    latent,
    context,
    cond,
    cond_context,
    mod_weight,
    norm_gain,
    down_q,
    down_kv,
    rope_weight,
    qlat_gain,
    kvlat_gain,
    up_query,
    up_key,
    up_value,
    query_gain,
    key_gain,
    context_bias,
    out_weight,
):
    seq_index = lax.axis_index("sp")
    tp_count = lax.axis_size("tp")
    own_rows = latent.shape[0]
    block_tokens = own_rows * tp_count
    row_span = mod_weight.shape[1]
    activated = jax.nn.silu(jnp.stack([cond, cond_context]).astype(jnp.float32)).astype(
        jnp.bfloat16
    )
    own_part = lax.dynamic_slice_in_dim(activated, seq_index * row_span, row_span, 1)
    partial_value = jnp.concatenate(
        [
            jnp.einsum("d,rde->re", own_part[0], mod_weight, preferred_element_type=jnp.float32),
            jnp.einsum(
                "d,rde->re", own_part[1], mod_weight[:2], preferred_element_type=jnp.float32
            ),
        ],
        axis=0,
    )
    summed = lax.psum(partial_value, "sp")
    modulations = lax.all_gather(summed, "tp", axis=1, tiled=True)
    normed = modulate(latent, norm_gain, modulations[0], modulations[1])
    context_normed = modulate(context, norm_gain, modulations[3], modulations[4])
    stacked = jnp.concatenate([normed, context_normed], axis=0)
    pieces = (
        lax.all_gather(down_q, "tp", axis=0, tiled=True),
        lax.all_gather(down_kv, "tp", axis=0, tiled=True),
    )
    columns = stacked
    query_down = jnp.dot(columns[:own_rows], pieces[0], preferred_element_type=jnp.float32)
    kv_down = jnp.dot(columns, pieces[1], preferred_element_type=jnp.float32)
    query_latent = rms_scale(query_down, qlat_gain).astype(jnp.bfloat16)
    kv_latent = rms_scale(kv_down, kvlat_gain).astype(jnp.bfloat16)
    rope_rows = jnp.dot(stacked, rope_weight, preferred_element_type=jnp.float32).astype(
        jnp.bfloat16
    )
    all_query, all_kv, all_rope = (
        lax.all_gather(query_latent, "tp", axis=0, tiled=True),
        lax.all_gather(kv_latent[:own_rows], "tp", axis=0, tiled=True),
        lax.all_gather(rope_rows[:own_rows], "tp", axis=0, tiled=True),
    )
    own_context_keys, own_context_values = make_keys(
        kv_latent[own_rows:], rope_rows[own_rows:], up_key, up_value, key_gain, None
    )
    context_keys, context_values = (
        lax.all_gather(own_context_keys, "sp", axis=0, tiled=True),
        lax.all_gather(own_context_values, "sp", axis=0, tiled=True),
    )
    positions = seq_index * block_tokens + jnp.arange(block_tokens, dtype=jnp.int32)
    tables = axial_tables(positions)
    queries = make_queries(all_query, up_query, query_gain, tables)
    keys, values = make_keys(all_kv, all_rope, up_key, up_value, key_gain, tables)
    head_count = queries.shape[1]
    shift_heads = context_bias + math.log(TOK_DEV / CTX_DEV)
    start_state = (
        jnp.full((block_tokens, head_count), -jnp.inf, jnp.float32),
        jnp.zeros((block_tokens, head_count), jnp.float32),
        jnp.zeros((block_tokens, head_count, VDIM), jnp.float32),
    )
    state_now = absorb_block(start_state, queries, context_keys, context_values, shift_heads)
    no_shift = jnp.zeros((head_count,), jnp.float32)
    pieces = (
        lax.all_gather(keys, "sp", axis=0, tiled=True),
        lax.all_gather(values, "sp", axis=0, tiled=True),
    )
    amount = pieces[0].shape[0]
    span_rows = math.gcd(amount, 1024)
    key_blocks = pieces[0].reshape(amount // span_rows, span_rows, head_count, pieces[0].shape[2])
    value_blocks = pieces[1].reshape(amount // span_rows, span_rows, head_count, pieces[1].shape[2])

    def scan_step(state_mid, blocks):
        return (absorb_block(state_mid, queries, blocks[0], blocks[1], no_shift), None)

    state_out, unused = lax.scan(scan_step, state_now, (key_blocks, value_blocks))
    run_max, run_sum, run_acc = state_out
    attended = (
        (run_acc / run_sum[..., None]).astype(jnp.bfloat16).reshape(block_tokens, head_count * VDIM)
    )
    token_rows = lax.all_to_all(attended, "tp", split_axis=0, concat_axis=1, tiled=True)
    columns = token_rows
    projected = jnp.dot(
        columns,
        lax.all_gather(out_weight, "tp", axis=0, tiled=True),
        preferred_element_type=jnp.float32,
    )
    return (latent.astype(jnp.float32) + modulations[2] * projected).astype(jnp.bfloat16)


def solution(mesh):
    in_specs = (
        P(("sp", "tp"), None),
        P("sp", None),
        P(),
        P(),
        P(None, "sp", "tp"),
        P(),
        P("tp", None),
        P("tp", None),
        P(),
        P(),
        P(),
        P(None, "tp"),
        P(None, "tp"),
        P(None, "tp"),
        P(),
        P(),
        P("tp"),
        P("tp", None),
    )
    out_specs = P(("sp", "tp"), None)
    return jax.shard_map(shards, mesh=mesh, in_specs=in_specs, out_specs=out_specs, check_vma=False)
```

profile of v0, /device:TPU:0, one launch (start us, length us, event | category | flops | bytes accessed | tf_op | source)
XLA Modules:
  0.0 254.6 jit_solution(11585700958939711861)
XLA Ops:
  6.5 0.7 all-gather.8.cloned.1.call-update
  7.3 0.7 all-gather.10.cloned.1.call-update
  8.1 0.7 stack.10
  8.8 0.7 stack.9
  9.5 1.3 fusion.62
  10.9 1.2 fusion.33
  12.1 0.7 convert_element_type.90
  12.8 0.7 convert_element_type.94
  13.5 11.5 %psum.7 = f32[5,256]{1,0:T(8,128)S(1)} all-reduce(f32[5,256]{1,0:T(8,128)S(1)} %pad_maximum_fusion.5), channel_id=1, replica_groups=mesh['sp'=4,'tp'=8] {'sp'}, use_global_device_ids=true, to_apply=%region_0.1 | all-reduce | flops 1280 | bytes 10240 | tf_op jit(solution)/shard_map/psum | solution.py:144
  25.0 14.7 %all_gather.33 = f32[5,2048]{1,0:T(8,128)S(1)} all-gather(f32[5,256]{1,0:T(8,128)S(1)} %psum.7), channel_id=1, replica_groups=mesh['sp'=4,'tp'=8] {'tp'}, dimensions={1}, use_global_device_ids=true | all-gather | bytes 46080 | tf_op jit(solution)/shard_map/all_gather | solution.py:145
  39.7 1.0 fusion.36
  40.7 1.2 fusion.24
  42.0 1.0 fusion.40
  43.1 1.3 fusion.28
  44.4 2.2 multiply_reduce_fusion.3
  46.7 0.1 multiply_convert_fusion.1
  46.8 0.7 slice.86
  47.6 33.1 %all-gather.10.cloned.1.call-done = bf16[2048,768]{1,0:T(8,128)(2,1)} async-done(((bf16[256,768]{1,0:T(8,128)(2,1)}), bf16[2048,768]{1,0:T(8,128)(2,1)}) %all-gather.10.cloned.1.call-update) | async-done | bytes 3145744 | tf_op jit(solution)/shard_map/all_gather | solution.py:150
  80.7 2.6 %multiply_reduce_fusion.2 = (f32[128]{0:T(128)S(1)}, f32[128,768]{1,0:T(8,128)S(1)}) fusion(bf16[128,2048]{1,0:T(8,128)(2,1)S(1)} %fusion.28, bf16[2048,768]{1,0:T(8,128)(2,1)} %all-gather.10.cloned.1.call-done), kind=kOutput, calls=%fused_computation.55 | convolution fusion | flops 402849664 | bytes 4063744 | tf_op jit(solution)/shard_map/dot_general | solution.py:154
  83.2 0.8 multiply_convert_fusion
  84.1 0.3 convolution_convert_fusion.1
  84.4 13.1 %all_gather.40 = bf16[1024,32]{0,1:T(8,128)(2,1)S(1)} all-gather(bf16[128,32]{0,1:T(8,128)(2,1)S(1)} %slice.87), channel_id=1, replica_groups=mesh['sp'=4,'tp'=8] {'tp'}, dimensions={0}, use_global_device_ids=true | all-gather | bytes 73728 | tf_op jit(solution)/shard_map/all_gather | solution.py:164
  97.6 0.3 multiply_cosine_fusion
  97.9 5.5 %all-gather.14.cloned.1.call-done = bf16[1024,512]{1,0:T(8,128)(2,1)} async-done(((bf16[128,512]{1,0:T(8,128)(2,1)}), bf16[1024,512]{1,0:T(8,128)(2,1)}) %all-gather.14.cloned.1.call-update) | async-done | bytes 1048592 | tf_op jit(solution)/shard_map/all_gather | solution.py:163
  103.4 1.8 fusion.69
  105.4 0.1 multiply_multiply_fusion
  105.6 1.2 convolution_convert_fusion
  106.8 23.0 %all-gather.12.cloned.1.call-done = bf16[1024,768]{1,0:T(8,128)(2,1)} async-done(((bf16[128,768]{1,0:T(8,128)(2,1)}), bf16[1024,768]{1,0:T(8,128)(2,1)}) %all-gather.12.cloned.1.call-update) | async-done | bytes 1572880 | tf_op jit(solution)/shard_map/all_gather | solution.py:162
  129.8 2.1 fusion.68
  132.0 0.1 multiply_multiply_fusion.1
  132.3 0.7 copy-done.3
  133.1 0.7 all-gather.20.cloned.1.call-update
  133.9 0.1 fusion.52
  134.0 0.1 convolution_convert_fusion.2
  134.2 0.1 reshape.230
  134.3 0.2 multiply_reduce_fusion.4
  134.5 0.1 multiply_convert_fusion.2
  134.6 8.7 %all_gather.35 = bf16[128,2,96]{2,0,1:T(8,128)(2,1)S(1)} all-gather(bf16[32,2,96]{2,0,1:T(8,128)(2,1)S(1)} %multiply_convert_fusion.2), channel_id=1, replica_groups=mesh['sp'=4,'tp'=8] {'sp'}, dimensions={0}, use_global_device_ids=true | all-gather | bytes 61440 | tf_op jit(solution)/shard_map/all_gather | solution.py:170
  143.2 0.1 convert_element_type.104
  143.3 8.2 %all_gather.38 = bf16[128,2,64]{2,0,1:T(8,128)(2,1)S(1)} all-gather(bf16[32,2,64]{2,0,1:T(8,128)(2,1)S(1)} %copy.43), channel_id=1, replica_groups=mesh['sp'=4,'tp'=8] {'sp'}, dimensions={0}, use_global_device_ids=true | all-gather | bytes 40960 | tf_op jit(solution)/shard_map/all_gather | solution.py:171
  151.6 5.9 %all-gather.18.cloned.1.call-done = bf16[4096,2,64]{0,2,1:T(8,128)(2,1)} async-done(((bf16[1024,2,64]{0,2,1:T(8,128)(2,1)}), bf16[4096,2,64]{0,2,1:T(8,128)(2,1)}) %all-gather.18.cloned.1.call-update) | async-done | bytes 1048592 | tf_op jit(solution)/shard_map/all_gather | solution.py:188
  157.4 2.3 copy.60
  159.7 0.3 fusion.67
  160.0 0.2 fusion.30
  160.2 0.3 fusion.23
  160.5 29.4 %all-gather.16.cloned.1.call-done = bf16[4096,2,96]{0,2,1:T(8,128)(2,1)} async-done(((bf16[1024,2,96]{0,2,1:T(8,128)(2,1)}), bf16[4096,2,96]{0,2,1:T(8,128)(2,1)}) %all-gather.16.cloned.1.call-update) | async-done | bytes 1572880 | tf_op jit(solution)/shard_map/all_gather | solution.py:187
  189.9 1.6 copy.59
  191.5 21.5 %while.14 = (s32[]{:T(128)}, f32[1024,2]{0,1:T(2,128)S(1)}, f32[1024,2]{0,1:T(2,128)S(1)}, f32[1024,2,64]{0,2,1:T(8,128)S(1)}, bf16[4,1024,2,96]{1,3,2,0:T(8,128...) while((s32[]{:T(128)}, f32[1024,2]{0,1:T(2,128)S(1)}, ...), condition=%wide.region_13.14_spmd, body=%wide.region_10.13_spmd.sunk | while | flops 688132096 | bytes 27394648 | solution.py:198
  191.5 1.3 bitcast_reduce_fusion.2
  192.9 1.4 fusion.97
  194.3 2.6 %fusion.98 = f32[1024,2,64]{0,2,1:T(8,128)S(1)} fusion(f32[2,1024,1024]{2,1,0:T(8,128)S(1)} %get-tuple-element.168, f32[1024,2]{0,1:T(2,128)S(1)} %max.4, f32[1024,2,64]{0,2,1:T(8,128)S(1)} %get-tuple-element.182, bf16[4,1024,2,64]{1,3,2,0:T(8,128)(2,1)} %get-tuple-element.193, s32[]{:T(128)} %get-tuple-element.179, f32[1024,2]{0,1:T(2,128)S(1)} %get-tuple-element.170), kind=kOutput, calls=%fused_computation.7.clone.1 | convolution fusion | flops 274989056 | bytes 9716224 | tf_op jit(solution)/shard_map/while/body/eval_jaxpr/qhk,khd->qhd/dot_general | solution.py:97
  196.9 1.3 bitcast_reduce_fusion.2
  198.2 1.4 fusion.97
  199.6 2.6 %fusion.98 = f32[1024,2,64]{0,2,1:T(8,128)S(1)} fusion(f32[2,1024,1024]{2,1,0:T(8,128)S(1)} %get-tuple-element.168, f32[1024,2]{0,1:T(2,128)S(1)} %max.4, f32[1024,2,64]{0,2,1:T(8,128)S(1)} %get-tuple-element.182, bf16[4,1024,2,64]{1,3,2,0:T(8,128)(2,1)} %get-tuple-element.193, s32[]{:T(128)} %get-tuple-element.179, f32[1024,2]{0,1:T(2,128)S(1)} %get-tuple-element.170), kind=kOutput, calls=%fused_computation.7.clone.1 | convolution fusion | flops 274989056 | bytes 9716224 | tf_op jit(solution)/shard_map/while/body/eval_jaxpr/qhk,khd->qhd/dot_general | solution.py:97
  202.3 1.3 bitcast_reduce_fusion.2
  203.6 1.4 fusion.97
  205.0 2.6 %fusion.98 = f32[1024,2,64]{0,2,1:T(8,128)S(1)} fusion(f32[2,1024,1024]{2,1,0:T(8,128)S(1)} %get-tuple-element.168, f32[1024,2]{0,1:T(2,128)S(1)} %max.4, f32[1024,2,64]{0,2,1:T(8,128)S(1)} %get-tuple-element.182, bf16[4,1024,2,64]{1,3,2,0:T(8,128)(2,1)} %get-tuple-element.193, s32[]{:T(128)} %get-tuple-element.179, f32[1024,2]{0,1:T(2,128)S(1)} %get-tuple-element.170), kind=kOutput, calls=%fused_computation.7.clone.1 | convolution fusion | flops 274989056 | bytes 9716224 | tf_op jit(solution)/shard_map/while/body/eval_jaxpr/qhk,khd->qhd/dot_general | solution.py:97
  207.7 1.3 bitcast_reduce_fusion.2
  209.0 1.4 fusion.97
  210.4 2.6 %fusion.98 = f32[1024,2,64]{0,2,1:T(8,128)S(1)} fusion(f32[2,1024,1024]{2,1,0:T(8,128)S(1)} %get-tuple-element.168, f32[1024,2]{0,1:T(2,128)S(1)} %max.4, f32[1024,2,64]{0,2,1:T(8,128)S(1)} %get-tuple-element.182, bf16[4,1024,2,64]{1,3,2,0:T(8,128)(2,1)} %get-tuple-element.193, s32[]{:T(128)} %get-tuple-element.179, f32[1024,2]{0,1:T(2,128)S(1)} %get-tuple-element.170), kind=kOutput, calls=%fused_computation.7.clone.1 | convolution fusion | flops 274989056 | bytes 9716224 | tf_op jit(solution)/shard_map/while/body/eval_jaxpr/qhk,khd->qhd/dot_general | solution.py:97
  213.1 0.7 copy.47
  213.9 4.6 %all-to-all-start = ((bf16[8,128,128]{1,2,0:T(8,128)(2,1)}), bf16[8,128,128]{1,2,0:T(8,128)(2,1)S(1)}, u32[]{:S(2)}, u32[]{:S(2)}) async-start(bf16[8,128,128]{1,2,0:T(8,128)(2,1)} %copy.47), calls=%async_computation | async-start | bytes 524288 | tf_op jit(solution)/shard_map/all_to_all | solution.py:203
  218.5 25.6 %all-gather.20.cloned.1.call-done = bf16[1024,2048]{1,0:T(8,128)(2,1)} async-done(((bf16[128,2048]{1,0:T(8,128)(2,1)}), bf16[1024,2048]{1,0:T(8,128)(2,1)}) %all-gather.20.cloned.1.call-update) | async-done | bytes 4194320 | tf_op jit(solution)/shard_map/all_gather | solution.py:207
  244.1 3.7 %fusion.20 = bf16[128,2048]{1,0:T(8,128)(2,1)} fusion(bf16[128,1024]{0,1:T(8,128)(2,1)S(1)} %bitcast.112, bf16[1024,2048]{1,0:T(8,128)(2,1)} %all-gather.20.cloned.1.call-done, bf16[128,2048]{1,0:T(8,128)(2,1)S(1)} %copy-done.1, f32[2048]{0:T(1024)S(1)} %bitcast.113), kind=kOutput, calls=%fused_computation.20 | convolution fusion | flops 537919488 | bytes 5513216 | tf_op jit(solution)/shard_map/dot_general | solution.py:205
  (81 shorter events, 1.3 us)
Async XLA Ops:
  6.5 123.3 %copy-start = (bf16[768,192]{0,1:T(8,128)(2,1)S(1)}, bf16[768,192]{0,1:T(8,128)(2,1)}, u32[]{:S(2)}) copy-start(bf16[768,192]{0,1:T(8,128)(2,1)} %param.31) | copy-start | bytes 884740
  6.5 37.9 %all-gather.8.cloned.1.call-start = ((), (), s32[]{:S(2)}) async-start(), calls=%async_computation.1 | async-start | bytes 2359296 | tf_op jit(solution)/shard_map/all_gather | solution.py:151
  7.3 40.3 %copy-start.7 = (bf16[768]{0:T(1024)(128)(2,1)S(1)}, bf16[768]{0:T(1024)(128)(2,1)}, u32[]{:S(2)}) copy-start(bf16[768]{0:T(1024)(128)(2,1)} %param.29) | copy-start | bytes 4612
  7.3 73.4 %all-gather.10.cloned.1.call-start = ((), (), s32[]{:S(2)}) async-start(), calls=%async_computation.2 | async-start | bytes 3538944 | tf_op jit(solution)/shard_map/all_gather | solution.py:150
  8.0 95.4 %all-gather.14.cloned.1.call-start = ((), (), s32[]{:S(2)}) async-start(), calls=%async_computation.4 | async-start | bytes 1179648 | tf_op jit(solution)/shard_map/all_gather | solution.py:163
  44.4 39.7 %copy-start.9 = (bf16[2048,32]{0,1:T(8,128)(2,1)S(1)}, bf16[2048,32]{0,1:T(8,128)(2,1)}, u32[]{:S(2)}) copy-start(bf16[2048,32]{0,1:T(8,128)(2,1)} %param.28) | copy-start | bytes 393220
  46.7 56.7 %copy-start.4 = (bf16[512,128]{1,0:T(8,128)(2,1)S(1)}, bf16[512,128]{1,0:T(8,128)(2,1)}, u32[]{:S(2)}) copy-start(bf16[512,128]{1,0:T(8,128)(2,1)} %param.32) | copy-start | bytes 393220
  47.5 82.3 %all-gather.12.cloned.1.call-start = ((), (), s32[]{:S(2)}) async-start(), calls=%async_computation.3 | async-start | bytes 1769472 | tf_op jit(solution)/shard_map/all_gather | solution.py:162
  47.5 57.8 %copy-start.6 = (f32[96]{0:T(128)S(1)}, f32[96]{0:T(128)}, u32[]{:S(2)}) copy-start(f32[96]{0:T(128)} %param.35) | copy-start | bytes 1156
  83.2 22.3 %copy-start.5 = (bf16[512,128]{1,0:T(8,128)(2,1)S(1)}, bf16[512,128]{1,0:T(8,128)(2,1)}, u32[]{:S(2)}) copy-start(bf16[512,128]{1,0:T(8,128)(2,1)} %param.33) | copy-start | bytes 393220
  84.0 73.4 %all-gather.18.cloned.1.call-start = ((), (), s32[]{:S(2)}) async-start(), calls=%async_computation.6 | async-start | bytes 1310720 | tf_op jit(solution)/shard_map/all_gather | solution.py:188
  103.4 2.1 copy-start.2
  105.2 26.8 %copy-start.8 = (f32[96]{0:T(128)S(1)}, f32[96]{0:T(128)}, u32[]{:S(2)}) copy-start(f32[96]{0:T(128)} %param.34) | copy-start | bytes 1156
  106.7 27.1 %copy-start.10 = (f32[2]{0:T(128)S(1)}, f32[2]{0:T(128)}, u32[]{:S(2)}) copy-start(f32[2]{0:T(128)} %param.36) | copy-start | bytes 28
  106.8 83.2 %all-gather.16.cloned.1.call-start = ((), (), s32[]{:S(2)}) async-start(), calls=%async_computation.5 | async-start | bytes 1966080 | tf_op jit(solution)/shard_map/all_gather | solution.py:187
  132.3 0.7 copy-start.3
  133.1 111.0 %all-gather.20.cloned.1.call-start = ((), (), s32[]{:S(2)}) async-start(), calls=%async_computation.7 | async-start | bytes 4718592 | tf_op jit(solution)/shard_map/all_gather | solution.py:207
  191.5 52.5 %copy-start.1 = (bf16[128,2048]{1,0:T(8,128)(2,1)S(1)}, bf16[128,2048]{1,0:T(8,128)(2,1)}, u32[]{:S(2)}) copy-start(bf16[128,2048]{1,0:T(8,128)(2,1)} %param.20) | copy-start | bytes 1572868
  213.9 30.2 %all-to-all-start = ((bf16[8,128,128]{1,2,0:T(8,128)(2,1)}), bf16[8,128,128]{1,2,0:T(8,128)(2,1)S(1)}, u32[]{:S(2)}, u32[]{:S(2)}) async-start(bf16[8,128,128]{1,2,0:T(8,128)(2,1)} %copy.47), calls=%async_computation | async-start | bytes 524288 | tf_op jit(solution)/shard_map/all_to_all | solution.py:203
Sparse Core Ops, SparseCore 0:
  8.9 32.3 all-gather.7
  43.0 37.5 all-gather.9
  82.3 21.0 all-gather.13
  104.9 24.8 all-gather.11
  131.5 25.8 all-gather.17
  159.1 30.7 all-gather.15
  191.5 52.4 all-gather.19
where the time goes:
time: 256 us; the launch traced here: 255 us
  waiting for transfers between devices  125 us (49%)
  blocking collectives  56.2 us (22%)
  matrix products  33 us (13%)
  other arithmetic  14 us (5%)
  between operations  13.9 us (5%)
  local copies, waits for them, and re-layouts  7.88 us (3%)
  starting transfers between devices  4.82 us (2%)
    all_gather x1, waiting for transfers between devices, shards(): lax.all_gather(down_q, 'tp', axis=0, tiled=True)  33.1 us
    all_gather x1, waiting for transfers between devices, shards(): lax.all_gather(keys, 'sp', axis=0, tiled=True)  29.4 us
    all_gather x1, waiting for transfers between devices, shards(): lax.all_gather(out_weight, 'tp', axis=0, tiled=True)  25.6 us
    all_gather x1, waiting for transfers between devices, shards(): lax.all_gather(query_latent, 'tp', axis=0, tiled=True)  23 us
    all_gather x1, blocking collectives, shards(): modulations = lax.all_gather(summed, 'tp', axis=1, tiled=True)  14.7 us
    all_gather x1, blocking collectives, shards(): lax.all_gather(rope_rows[:own_rows], 'tp', axis=0, tiled=True)  13.1 us
    psum x1, blocking collectives, shards(): summed = lax.psum(partial_value, 'sp')  11.5 us
    dot_general x5, matrix products, absorb_block(): jnp.einsum('qhk,khd->qhd', weights.astype(jnp.bfloat16), value_block, pre...  10.7 us
  transfers between devices with their start and end apart: 8, of which 6 were waited for; matrix products, arithmetic and copies ran while one was open for 20% of the time, Pallas kernels for 0%

commit v1 on v0

--- a/solution.py
+++ b/solution.py
@@ -142,7 +142,7 @@
         axis=0,
     )
     summed = lax.psum(partial_value, "sp")
-    modulations = lax.all_gather(summed, "tp", axis=1, tiled=True)
+    modulations = jnp.concatenate(lax.all_gather(summed, "tp"), axis=1)
     normed = modulate(latent, norm_gain, modulations[0], modulations[1])
     context_normed = modulate(context, norm_gain, modulations[3], modulations[4])
     stacked = jnp.concatenate([normed, context_normed], axis=0)

time: 256 us -> 256 us (level)
  no operation moved by 1% of the time
where the time goes in v1:
time: 256 us; the launch traced here: 255 us
  waiting for transfers between devices  125 us (49%)
  blocking collectives  56.2 us (22%)
  matrix products  33 us (13%)
  other arithmetic  14 us (5%)
  between operations  13.9 us (5%)
  local copies, waits for them, and re-layouts  7.88 us (3%)
  starting transfers between devices  4.82 us (2%)
    all_gather x1, waiting for transfers between devices, shards(): lax.all_gather(down_q, 'tp', axis=0, tiled=True)  33.1 us
    all_gather x1, waiting for transfers between devices, shards(): lax.all_gather(keys, 'sp', axis=0, tiled=True)  29.4 us
    all_gather x1, waiting for transfers between devices, shards(): lax.all_gather(out_weight, 'tp', axis=0, tiled=True)  25.6 us
    all_gather x1, waiting for transfers between devices, shards(): lax.all_gather(query_latent, 'tp', axis=0, tiled=True)  23 us
    all_gather x1, blocking collectives, shards(): modulations = jnp.concatenate(lax.all_gather(summed, 'tp'), axis=1)  14.7 us
    all_gather x1, blocking collectives, shards(): lax.all_gather(rope_rows[:own_rows], 'tp', axis=0, tiled=True)  13.1 us
    psum x1, blocking collectives, shards(): summed = lax.psum(partial_value, 'sp')  11.5 us
    dot_general x5, matrix products, absorb_block(): jnp.einsum('qhk,khd->qhd', weights.astype(jnp.bfloat16), value_block, pre...  10.7 us
  transfers between devices with their start and end apart: 8, of which 6 were waited for; matrix products, arithmetic and copies ran while one was open for 20% of the time, Pallas kernels for 0%

profile of v1, /device:TPU:0, one launch (start us, length us, event | category | flops | bytes accessed | tf_op | source)
XLA Modules:
  0.0 254.6 jit_solution(13016957012956123958)
XLA Ops:
  6.5 0.7 all-gather.8.cloned.1.call-update
  7.3 0.7 all-gather.10.cloned.1.call-update
  8.1 0.7 stack.10
  8.8 0.7 stack.9
  9.5 1.3 fusion.62
  10.9 1.2 fusion.33
  12.1 0.7 convert_element_type.90
  12.8 0.7 convert_element_type.94
  13.5 11.5 %psum.7 = f32[1,5,256]{2,1,0:T(8,128)S(1)} all-reduce(f32[1,5,256]{2,1,0:T(8,128)S(1)} %maximum_bitcast_fusion), channel_id=1, replica_groups=mesh['sp'=4,'tp'=8] {'sp'}, use_global_device_ids=true, to_apply=%region_0.1 | all-reduce | flops 1280 | bytes 10240 | tf_op jit(solution)/shard_map/psum | solution.py:144
  25.0 14.7 %all_gather.37 = f32[8,5,256]{2,1,0:T(8,128)S(1)} all-gather(f32[1,5,256]{2,1,0:T(8,128)S(1)} %psum.7), channel_id=1, replica_groups=mesh['sp'=4,'tp'=8] {'tp'}, dimensions={0}, use_global_device_ids=true | all-gather | bytes 46080 | tf_op jit(solution)/shard_map/all_gather | solution.py:145
  39.7 1.0 fusion.36
  40.7 1.2 fusion.24
  42.0 1.0 fusion.40
  43.1 1.3 fusion.28
  44.4 2.2 multiply_reduce_fusion.3
  46.7 0.1 multiply_convert_fusion.1
  46.8 0.7 slice.91
  47.6 33.1 %all-gather.10.cloned.1.call-done = bf16[2048,768]{1,0:T(8,128)(2,1)} async-done(((bf16[256,768]{1,0:T(8,128)(2,1)}), bf16[2048,768]{1,0:T(8,128)(2,1)}) %all-gather.10.cloned.1.call-update) | async-done | bytes 3145744 | tf_op jit(solution)/shard_map/all_gather | solution.py:150
  80.7 2.6 %multiply_reduce_fusion.2 = (f32[128]{0:T(128)S(1)}, f32[128,768]{1,0:T(8,128)S(1)}) fusion(bf16[128,2048]{1,0:T(8,128)(2,1)S(1)} %fusion.28, bf16[2048,768]{1,0:T(8,128)(2,1)} %all-gather.10.cloned.1.call-done), kind=kOutput, calls=%fused_computation.55 | convolution fusion | flops 402849664 | bytes 4063744 | tf_op jit(solution)/shard_map/dot_general | solution.py:154
  83.2 0.8 multiply_convert_fusion
  84.1 0.3 convolution_convert_fusion.1
  84.4 13.1 %all_gather.44 = bf16[1024,32]{0,1:T(8,128)(2,1)S(1)} all-gather(bf16[128,32]{0,1:T(8,128)(2,1)S(1)} %slice.92), channel_id=1, replica_groups=mesh['sp'=4,'tp'=8] {'tp'}, dimensions={0}, use_global_device_ids=true | all-gather | bytes 73728 | tf_op jit(solution)/shard_map/all_gather | solution.py:164
  97.6 0.3 multiply_cosine_fusion
  97.9 5.5 %all-gather.14.cloned.1.call-done = bf16[1024,512]{1,0:T(8,128)(2,1)} async-done(((bf16[128,512]{1,0:T(8,128)(2,1)}), bf16[1024,512]{1,0:T(8,128)(2,1)}) %all-gather.14.cloned.1.call-update) | async-done | bytes 1048592 | tf_op jit(solution)/shard_map/all_gather | solution.py:163
  103.4 1.8 fusion.69
  105.3 0.1 multiply_multiply_fusion
  105.5 1.2 convolution_convert_fusion
  106.8 23.0 %all-gather.12.cloned.1.call-done = bf16[1024,768]{1,0:T(8,128)(2,1)} async-done(((bf16[128,768]{1,0:T(8,128)(2,1)}), bf16[1024,768]{1,0:T(8,128)(2,1)}) %all-gather.12.cloned.1.call-update) | async-done | bytes 1572880 | tf_op jit(solution)/shard_map/all_gather | solution.py:162
  129.8 2.1 fusion.68
  132.0 0.1 multiply_multiply_fusion.1
  132.3 0.7 copy-done.3
  133.1 0.7 all-gather.20.cloned.1.call-update
  133.9 0.1 fusion.52
  134.0 0.1 convolution_convert_fusion.2
  134.2 0.1 reshape.259
  134.3 0.2 multiply_reduce_fusion.4
  134.5 0.1 multiply_convert_fusion.2
  134.6 8.7 %all_gather.39 = bf16[128,2,96]{2,0,1:T(8,128)(2,1)S(1)} all-gather(bf16[32,2,96]{2,0,1:T(8,128)(2,1)S(1)} %multiply_convert_fusion.2), channel_id=1, replica_groups=mesh['sp'=4,'tp'=8] {'sp'}, dimensions={0}, use_global_device_ids=true | all-gather | bytes 61440 | tf_op jit(solution)/shard_map/all_gather | solution.py:170
  143.2 0.1 convert_element_type.104
  143.3 8.2 %all_gather.42 = bf16[128,2,64]{2,0,1:T(8,128)(2,1)S(1)} all-gather(bf16[32,2,64]{2,0,1:T(8,128)(2,1)S(1)} %copy.43), channel_id=1, replica_groups=mesh['sp'=4,'tp'=8] {'sp'}, dimensions={0}, use_global_device_ids=true | all-gather | bytes 40960 | tf_op jit(solution)/shard_map/all_gather | solution.py:171
  151.6 5.9 %all-gather.18.cloned.1.call-done = bf16[4096,2,64]{0,2,1:T(8,128)(2,1)} async-done(((bf16[1024,2,64]{0,2,1:T(8,128)(2,1)}), bf16[4096,2,64]{0,2,1:T(8,128)(2,1)}) %all-gather.18.cloned.1.call-update) | async-done | bytes 1048592 | tf_op jit(solution)/shard_map/all_gather | solution.py:188
  157.4 2.3 copy.60
  159.7 0.3 fusion.67
  160.0 0.2 fusion.30
  160.2 0.3 fusion.23
  160.5 29.4 %all-gather.16.cloned.1.call-done = bf16[4096,2,96]{0,2,1:T(8,128)(2,1)} async-done(((bf16[1024,2,96]{0,2,1:T(8,128)(2,1)}), bf16[4096,2,96]{0,2,1:T(8,128)(2,1)}) %all-gather.16.cloned.1.call-update) | async-done | bytes 1572880 | tf_op jit(solution)/shard_map/all_gather | solution.py:187
  189.9 1.6 copy.59
  191.5 21.5 %while.14 = (s32[]{:T(128)}, f32[1024,2]{0,1:T(2,128)S(1)}, f32[1024,2]{0,1:T(2,128)S(1)}, f32[1024,2,64]{0,2,1:T(8,128)S(1)}, bf16[4,1024,2,96]{1,3,2,0:T(8,128...) while((s32[]{:T(128)}, f32[1024,2]{0,1:T(2,128)S(1)}, ...), condition=%wide.region_13.14_spmd, body=%wide.region_10.13_spmd.sunk | while | flops 688132096 | bytes 27394648 | solution.py:198
  191.5 1.3 bitcast_reduce_fusion.2
  192.9 1.4 fusion.97
  194.3 2.6 %fusion.98 = f32[1024,2,64]{0,2,1:T(8,128)S(1)} fusion(f32[2,1024,1024]{2,1,0:T(8,128)S(1)} %get-tuple-element.168, f32[1024,2]{0,1:T(2,128)S(1)} %max.4, f32[1024,2,64]{0,2,1:T(8,128)S(1)} %get-tuple-element.182, bf16[4,1024,2,64]{1,3,2,0:T(8,128)(2,1)} %get-tuple-element.193, s32[]{:T(128)} %get-tuple-element.179, f32[1024,2]{0,1:T(2,128)S(1)} %get-tuple-element.170), kind=kOutput, calls=%fused_computation.7.clone.1 | convolution fusion | flops 274989056 | bytes 9716224 | tf_op jit(solution)/shard_map/while/body/eval_jaxpr/qhk,khd->qhd/dot_general | solution.py:97
  196.9 1.3 bitcast_reduce_fusion.2
  198.2 1.4 fusion.97
  199.6 2.6 %fusion.98 = f32[1024,2,64]{0,2,1:T(8,128)S(1)} fusion(f32[2,1024,1024]{2,1,0:T(8,128)S(1)} %get-tuple-element.168, f32[1024,2]{0,1:T(2,128)S(1)} %max.4, f32[1024,2,64]{0,2,1:T(8,128)S(1)} %get-tuple-element.182, bf16[4,1024,2,64]{1,3,2,0:T(8,128)(2,1)} %get-tuple-element.193, s32[]{:T(128)} %get-tuple-element.179, f32[1024,2]{0,1:T(2,128)S(1)} %get-tuple-element.170), kind=kOutput, calls=%fused_computation.7.clone.1 | convolution fusion | flops 274989056 | bytes 9716224 | tf_op jit(solution)/shard_map/while/body/eval_jaxpr/qhk,khd->qhd/dot_general | solution.py:97
  202.3 1.3 bitcast_reduce_fusion.2
  203.6 1.4 fusion.97
  205.0 2.6 %fusion.98 = f32[1024,2,64]{0,2,1:T(8,128)S(1)} fusion(f32[2,1024,1024]{2,1,0:T(8,128)S(1)} %get-tuple-element.168, f32[1024,2]{0,1:T(2,128)S(1)} %max.4, f32[1024,2,64]{0,2,1:T(8,128)S(1)} %get-tuple-element.182, bf16[4,1024,2,64]{1,3,2,0:T(8,128)(2,1)} %get-tuple-element.193, s32[]{:T(128)} %get-tuple-element.179, f32[1024,2]{0,1:T(2,128)S(1)} %get-tuple-element.170), kind=kOutput, calls=%fused_computation.7.clone.1 | convolution fusion | flops 274989056 | bytes 9716224 | tf_op jit(solution)/shard_map/while/body/eval_jaxpr/qhk,khd->qhd/dot_general | solution.py:97
  207.7 1.3 bitcast_reduce_fusion.2
  209.0 1.4 fusion.97
  210.4 2.6 %fusion.98 = f32[1024,2,64]{0,2,1:T(8,128)S(1)} fusion(f32[2,1024,1024]{2,1,0:T(8,128)S(1)} %get-tuple-element.168, f32[1024,2]{0,1:T(2,128)S(1)} %max.4, f32[1024,2,64]{0,2,1:T(8,128)S(1)} %get-tuple-element.182, bf16[4,1024,2,64]{1,3,2,0:T(8,128)(2,1)} %get-tuple-element.193, s32[]{:T(128)} %get-tuple-element.179, f32[1024,2]{0,1:T(2,128)S(1)} %get-tuple-element.170), kind=kOutput, calls=%fused_computation.7.clone.1 | convolution fusion | flops 274989056 | bytes 9716224 | tf_op jit(solution)/shard_map/while/body/eval_jaxpr/qhk,khd->qhd/dot_general | solution.py:97
  213.1 0.7 copy.47
  213.9 4.6 %all-to-all-start = ((bf16[8,128,128]{1,2,0:T(8,128)(2,1)}), bf16[8,128,128]{1,2,0:T(8,128)(2,1)S(1)}, u32[]{:S(2)}, u32[]{:S(2)}) async-start(bf16[8,128,128]{1,2,0:T(8,128)(2,1)} %copy.47), calls=%async_computation | async-start | bytes 524288 | tf_op jit(solution)/shard_map/all_to_all | solution.py:203
  218.5 25.6 %all-gather.20.cloned.1.call-done = bf16[1024,2048]{1,0:T(8,128)(2,1)} async-done(((bf16[128,2048]{1,0:T(8,128)(2,1)}), bf16[1024,2048]{1,0:T(8,128)(2,1)}) %all-gather.20.cloned.1.call-update) | async-done | bytes 4194320 | tf_op jit(solution)/shard_map/all_gather | solution.py:207
  244.1 3.7 %fusion.20 = bf16[128,2048]{1,0:T(8,128)(2,1)} fusion(bf16[128,1024]{0,1:T(8,128)(2,1)S(1)} %bitcast.115, bf16[1024,2048]{1,0:T(8,128)(2,1)} %all-gather.20.cloned.1.call-done, bf16[128,2048]{1,0:T(8,128)(2,1)S(1)} %copy-done.1, f32[2048]{0:T(1024)S(1)} %bitcast.117), kind=kOutput, calls=%fused_computation.20 | convolution fusion | flops 537919488 | bytes 5513216 | tf_op jit(solution)/shard_map/dot_general | solution.py:205
  (81 shorter events, 1.3 us)
Async XLA Ops:
  6.5 123.3 %copy-start = (bf16[768,192]{0,1:T(8,128)(2,1)S(1)}, bf16[768,192]{0,1:T(8,128)(2,1)}, u32[]{:S(2)}) copy-start(bf16[768,192]{0,1:T(8,128)(2,1)} %param.31) | copy-start | bytes 884740
  6.5 37.9 %all-gather.8.cloned.1.call-start = ((), (), s32[]{:S(2)}) async-start(), calls=%async_computation.1 | async-start | bytes 2359296 | tf_op jit(solution)/shard_map/all_gather | solution.py:151
  7.3 40.3 %copy-start.7 = (bf16[768]{0:T(1024)(128)(2,1)S(1)}, bf16[768]{0:T(1024)(128)(2,1)}, u32[]{:S(2)}) copy-start(bf16[768]{0:T(1024)(128)(2,1)} %param.29) | copy-start | bytes 4612
  7.3 73.4 %all-gather.10.cloned.1.call-start = ((), (), s32[]{:S(2)}) async-start(), calls=%async_computation.2 | async-start | bytes 3538944 | tf_op jit(solution)/shard_map/all_gather | solution.py:150
  8.0 95.4 %all-gather.14.cloned.1.call-start = ((), (), s32[]{:S(2)}) async-start(), calls=%async_computation.4 | async-start | bytes 1179648 | tf_op jit(solution)/shard_map/all_gather | solution.py:163
  44.4 39.7 %copy-start.9 = (bf16[2048,32]{0,1:T(8,128)(2,1)S(1)}, bf16[2048,32]{0,1:T(8,128)(2,1)}, u32[]{:S(2)}) copy-start(bf16[2048,32]{0,1:T(8,128)(2,1)} %param.28) | copy-start | bytes 393220
  46.7 56.7 %copy-start.4 = (bf16[512,128]{1,0:T(8,128)(2,1)S(1)}, bf16[512,128]{1,0:T(8,128)(2,1)}, u32[]{:S(2)}) copy-start(bf16[512,128]{1,0:T(8,128)(2,1)} %param.32) | copy-start | bytes 393220
  47.5 82.3 %all-gather.12.cloned.1.call-start = ((), (), s32[]{:S(2)}) async-start(), calls=%async_computation.3 | async-start | bytes 1769472 | tf_op jit(solution)/shard_map/all_gather | solution.py:162
  47.5 57.8 %copy-start.6 = (f32[96]{0:T(128)S(1)}, f32[96]{0:T(128)}, u32[]{:S(2)}) copy-start(f32[96]{0:T(128)} %param.35) | copy-start | bytes 1156
  83.2 22.3 %copy-start.5 = (bf16[512,128]{1,0:T(8,128)(2,1)S(1)}, bf16[512,128]{1,0:T(8,128)(2,1)}, u32[]{:S(2)}) copy-start(bf16[512,128]{1,0:T(8,128)(2,1)} %param.33) | copy-start | bytes 393220
  84.0 73.4 %all-gather.18.cloned.1.call-start = ((), (), s32[]{:S(2)}) async-start(), calls=%async_computation.6 | async-start | bytes 1310720 | tf_op jit(solution)/shard_map/all_gather | solution.py:188
  103.4 2.1 copy-start.2
  105.2 26.8 %copy-start.8 = (f32[96]{0:T(128)S(1)}, f32[96]{0:T(128)}, u32[]{:S(2)}) copy-start(f32[96]{0:T(128)} %param.34) | copy-start | bytes 1156
  106.7 27.2 %copy-start.10 = (f32[2]{0:T(128)S(1)}, f32[2]{0:T(128)}, u32[]{:S(2)}) copy-start(f32[2]{0:T(128)} %param.36) | copy-start | bytes 28
  106.8 83.2 %all-gather.16.cloned.1.call-start = ((), (), s32[]{:S(2)}) async-start(), calls=%async_computation.5 | async-start | bytes 1966080 | tf_op jit(solution)/shard_map/all_gather | solution.py:187
  132.3 0.7 copy-start.3
  133.1 111.0 %all-gather.20.cloned.1.call-start = ((), (), s32[]{:S(2)}) async-start(), calls=%async_computation.7 | async-start | bytes 4718592 | tf_op jit(solution)/shard_map/all_gather | solution.py:207
  191.5 52.5 %copy-start.1 = (bf16[128,2048]{1,0:T(8,128)(2,1)S(1)}, bf16[128,2048]{1,0:T(8,128)(2,1)}, u32[]{:S(2)}) copy-start(bf16[128,2048]{1,0:T(8,128)(2,1)} %param.20) | copy-start | bytes 1572868
  213.9 30.2 %all-to-all-start = ((bf16[8,128,128]{1,2,0:T(8,128)(2,1)}), bf16[8,128,128]{1,2,0:T(8,128)(2,1)S(1)}, u32[]{:S(2)}, u32[]{:S(2)}) async-start(bf16[8,128,128]{1,2,0:T(8,128)(2,1)} %copy.47), calls=%async_computation | async-start | bytes 524288 | tf_op jit(solution)/shard_map/all_to_all | solution.py:203
Sparse Core Ops, SparseCore 0:
  8.9 32.3 all-gather.7
  43.0 37.5 all-gather.9
  82.3 21.0 all-gather.13
  104.9 24.8 all-gather.11
  131.5 25.8 all-gather.17
  159.1 30.7 all-gather.15
  191.5 52.4 all-gather.19
